TPU v7x, 512 devices: a whole 4x8x8 slice. The times are simulated.
512 devices in a mesh: sp: 64 (over z, y), tp: 8 (over x, core).
Axes of the slice: x: 4, y: 8, z: 8, core: 2. Of those that a mesh axis runs over, the one named last changes fastest.
Arguments:
- latent_tokens: bfloat16 [8192, 2048], P(('sp', 'tp')), may hold values from -6 to 6
- context_tokens: bfloat16 [512, 2048], P('sp'), may hold values from -6 to 6
- cond: float32 [2048], replicated, may hold values from -6 to 6
- ctx_cond: float32 [2048], replicated, may hold values from -6 to 6
- mod_shift: bfloat16 [2048, 2048], P('sp', 'tp'), may hold values from -0.125 to 0.125
- mod_scale: bfloat16 [2048, 2048], P('sp', 'tp'), may hold values from -0.125 to 0.125
- mod_gate: bfloat16 [2048, 2048], P('sp', 'tp'), may hold values from -0.125 to 0.125
- norm_gain: float32 [2048], replicated, may hold values from 0.1 to 1.9
- w_query: bfloat16 [2048, 1536], P(None, 'tp'), may hold values from -0.125 to 0.125
- query_gain: float32 [96], replicated, may hold values from 0.8 to 2
- w_down_kv: bfloat16 [2048, 256], replicated, may hold values from -0.125 to 0.125
- w_rope_key: bfloat16 [2048, 32], replicated, may hold values from -0.125 to 0.125
- kv_gain: float32 [256], replicated, may hold values from 0.1 to 1.9
- w_up_kv: bfloat16 [2, 256, 1024], P(None, None, 'tp'), may hold values from -0.375 to 0.375
- key_gain: float32 [96], replicated, may hold values from 0.8 to 2
- ctx_lift: float32 [16], P('tp'), may hold values from 1.5 to 220
- w_output: bfloat16 [1024, 2048], P('tp'), may hold values from -0.1875 to 0.1875
Outputs:
- updated: bfloat16 [8192, 2048], P(('sp', 'tp'))
All inputs are finite; a program needn't handle non-finite values.
Results may differ from a plain program's by a relative error of at most 0.007.
Values may be sent and summed in bfloat16 or wider, within the bound.
A program may use at most 64 MiB of HBM per device.

v0:
```python
import functools
import jax
import jax.numpy as jnp
from jax import lax
from jax.sharding import Mesh
from jax.sharding import PartitionSpec as P

HD = 64
ROPE = 32
QK = 96
GRID_W = 64
SP = ("sp_0", "sp_1")
SP_TP = ("sp_0", "sp_1", "tp")
EPS = 1e-06
THETA = 10000.0


def over_axes(value, axes):
    return functools.reduce(lax.psum, axes, value)


def in_one_piece(arrays, axis, dim, along):
    ends, at = ([], 0)
    for a in arrays[:-1]:
        at += a.shape[along]
        ends.append(at)
    both = jnp.concatenate(arrays, axis=along)
    return tuple(jnp.split(lax.all_gather(both, axis, axis=dim, tiled=True), ends, axis=along))


def copy_for_each(value, axis):
    copies = jnp.broadcast_to(value, (lax.axis_size(axis), *value.shape))
    return lax.all_to_all(copies, axis, split_axis=0, concat_axis=0, tiled=True)


def joined_along(tiles, dim):
    tiles = jnp.moveaxis(tiles, 0, dim)
    shape = tiles.shape
    return tiles.reshape(*shape[:dim], shape[dim] * shape[dim + 1], *shape[dim + 2 :])


def collect(value, axis, dim):
    tiles = copy_for_each(value, axis)
    return joined_along(tiles, dim)


def split_up(value, dim, count):
    shape = value.shape
    tiles = value.reshape(*shape[:dim], count, shape[dim] // count, *shape[dim + 1 :])
    return jnp.moveaxis(tiles, dim, 0)


def sent_and_summed(value, axis, dim):
    count = lax.axis_size(axis)
    tiles = lax.all_to_all(split_up(value, dim, count), axis, 0, 0, tiled=True)
    return jnp.sum(tiles.astype(jnp.float32), axis=0)


def rms_normed(values, gain_vector):
    values = values.astype(jnp.float32)
    inv_root = lax.rsqrt(jnp.mean(values * values, axis=-1, keepdims=True) + EPS)
    return values * inv_root * gain_vector


def grid_angles(position, width):
    freq_count = width // 4
    inverse = THETA ** (-jnp.arange(freq_count, dtype=jnp.float32) / freq_count)
    row_index = (position // GRID_W).astype(jnp.float32)
    col_index = (position % GRID_W).astype(jnp.float32)
    return jnp.concatenate([row_index[:, None] * inverse, col_index[:, None] * inverse], axis=-1)


def rotate_tail(head_rows, angle, plain):
    tail = head_rows[..., plain:]
    half_width = tail.shape[-1] // 2
    cosine = jnp.cos(angle)[:, None, :]
    sine_val = jnp.sin(angle)[:, None, :]
    front_half = tail[..., :half_width]
    back_half = tail[..., half_width:]
    return jnp.concatenate(
        [
            head_rows[..., :plain],
            front_half * cosine - back_half * sine_val,
            back_half * cosine + front_half * sine_val,
        ],
        axis=-1,
    )


def modulation(signal, weight):
    return jnp.dot(signal, weight.astype(jnp.float32))


def compress(hidden, w_down_kv, w_rope_key, kv_gain):
    latent = rms_normed(jnp.dot(hidden, w_down_kv, preferred_element_type=jnp.float32), kv_gain)
    rope_key = jnp.dot(hidden, w_rope_key, preferred_element_type=jnp.float32)
    return (latent.astype(jnp.bfloat16), rope_key.astype(jnp.bfloat16))


def expand(latent, rope_key, w_up_kv, key_gain, angle):
    row_count = latent.shape[0]
    head_count = w_up_kv.shape[2] // HD
    key_plain = jnp.dot(latent, w_up_kv[0], preferred_element_type=jnp.float32).reshape(
        row_count, head_count, HD
    )
    shared = jnp.broadcast_to(
        rope_key.astype(jnp.float32)[:, None, :], (row_count, head_count, ROPE)
    )
    keys = rms_normed(jnp.concatenate([key_plain, shared], axis=-1), key_gain)
    if angle is not None:
        keys = rotate_tail(keys, angle, HD)
    values = jnp.dot(latent, w_up_kv[1], preferred_element_type=jnp.float32).astype(jnp.bfloat16)
    return (keys.astype(jnp.bfloat16), values.reshape(row_count, head_count, HD))


def absorb(carry, query_heads, keys, values, lift):
    highest, total, mixed = carry
    scores = (
        jnp.einsum("qhd,khd->hqk", query_heads, keys, preferred_element_type=jnp.float32)
        * QK ** (-0.5)
        + lift
    )
    new_high = jnp.maximum(highest, jnp.max(scores, axis=-1))
    weights = jnp.exp(scores - new_high[:, :, None])
    factor = jnp.exp(highest - new_high)
    total = total * factor + jnp.sum(weights, axis=-1)
    update = jnp.einsum(
        "hqk,khd->qhd", weights.astype(jnp.bfloat16), values, preferred_element_type=jnp.float32
    )
    mixed = mixed * jnp.transpose(factor)[:, :, None] + update
    return (new_high, total, mixed)


def local(
    latent_tokens,
    context_tokens,
    cond,
    ctx_cond,
    mod_shift,
    mod_scale,
    mod_gate,
    norm_gain,
    w_query,
    query_gain,
    w_down_kv,
    w_rope_key,
    kv_gain,
    w_up_kv,
    key_gain,
    ctx_lift,
    w_output,
):
    tp_count = lax.axis_size("tp")
    sp_index = lax.axis_index(SP)
    piece_rows = mod_shift.shape[0]
    own_start = sp_index * piece_rows
    lat_signal = jax.nn.silu(lax.dynamic_slice_in_dim(cond, own_start, piece_rows, 0))
    ctx_signal = jax.nn.silu(lax.dynamic_slice_in_dim(ctx_cond, own_start, piece_rows, 0))
    both_signal = jnp.stack([lat_signal, ctx_signal])
    shift_part = modulation(both_signal, mod_shift)
    scale_part = modulation(both_signal, mod_scale)
    gate_part = modulation(lat_signal[None, :], mod_gate)
    shift_sum, scale_sum, gate_sum = (
        over_axes(shift_part, SP),
        over_axes(scale_part, SP),
        over_axes(gate_part, SP),
    )
    shift_vec, scale_vec, gate_vec = in_one_piece((shift_sum, scale_sum, gate_sum), "tp", 1, 0)
    hidden_lat = (
        rms_normed(latent_tokens, norm_gain) * (1.0 + scale_vec[0]) + shift_vec[0]
    ).astype(jnp.bfloat16)
    ctx_rows = lax.all_gather(context_tokens, SP, axis=0, tiled=True)
    ctx_hidden = (rms_normed(ctx_rows, norm_gain) * (1.0 + scale_vec[1]) + shift_vec[1]).astype(
        jnp.bfloat16
    )
    ctx_latent, ctx_rope = compress(ctx_hidden, w_down_kv, w_rope_key, kv_gain)
    ctx_keys, ctx_values = expand(ctx_latent, ctx_rope, w_up_kv, key_gain, None)
    head_count = ctx_lift.shape[0]
    local_rows = latent_tokens.shape[0]
    group_rows = local_rows * tp_count
    group_start = sp_index * group_rows
    qk_width = head_count * QK
    piece = collect(hidden_lat, "tp", 0)
    row_count = piece.shape[0]
    position = group_start + jnp.arange(row_count, dtype=jnp.int32)
    latent, rope_key = compress(piece, w_down_kv, w_rope_key, kv_gain)
    keys, values = expand(latent, rope_key, w_up_kv, key_gain, grid_angles(position, ROPE))
    make_row_count = piece.shape[0]
    position = group_start + jnp.arange(make_row_count, dtype=jnp.int32)
    raw = jnp.dot(piece, w_query, preferred_element_type=jnp.float32).reshape(
        make_row_count, head_count, QK
    )
    turned = rotate_tail(rms_normed(raw, query_gain), grid_angles(position, ROPE), HD)
    projected = jnp.concatenate(
        [
            turned.astype(jnp.bfloat16).reshape(make_row_count, qk_width),
            keys.reshape(row_count, qk_width),
            values.reshape(row_count, head_count * HD),
        ],
        axis=1,
    )
    queries = projected[:, :qk_width]
    group_keys = projected[:, qk_width : 2 * qk_width]
    group_values = projected[:, 2 * qk_width :]
    query_heads = queries.reshape(group_rows, head_count, QK)
    start_carry = (
        jnp.full((head_count, group_rows), -1e30, jnp.float32),
        jnp.zeros((head_count, group_rows), jnp.float32),
        jnp.zeros((group_rows, head_count, HD), jnp.float32),
    )
    carry = absorb(start_carry, query_heads, ctx_keys, ctx_values, ctx_lift[:, None, None])
    pieces = in_one_piece((group_keys, group_values), SP, 0, 1)
    row_count = pieces[0].shape[0]
    keys = pieces[0].reshape(row_count, head_count, QK)
    values = pieces[1].reshape(row_count, head_count, HD)
    carry = absorb(carry, query_heads, keys, values, 0.0)
    highest, total, mixed = carry
    attended = (
        (mixed / jnp.transpose(total)[:, :, None])
        .astype(jnp.bfloat16)
        .reshape(group_rows, head_count * HD)
    )
    out = sent_and_summed(
        jnp.dot(attended, w_output, preferred_element_type=jnp.float32).astype(jnp.bfloat16),
        "tp",
        0,
    )
    return (latent_tokens.astype(jnp.float32) + gate_vec[0] * out).astype(jnp.bfloat16)


def solution(mesh):
    finer = Mesh(mesh.devices.reshape(8, 8, mesh.shape["tp"]), ("sp_0", "sp_1", "tp"))
    in_specs = (
        P(SP_TP, None),
        P(SP, None),
        P(),
        P(),
        P(SP, "tp"),
        P(SP, "tp"),
        P(SP, "tp"),
        P(),
        P(None, "tp"),
        P(),
        P(),
        P(),
        P(),
        P(None, None, "tp"),
        P(),
        P("tp"),
        P("tp", None),
    )
    out_specs = P(SP_TP, None)
    return jax.shard_map(local, mesh=finer, in_specs=in_specs, out_specs=out_specs, check_vma=False)
```

profile of v0, /device:TPU:1, one launch (start us, length us, event | category | flops | bytes accessed | tf_op | source)
XLA Modules:
  0.0 226.2 jit_solution(14526996260051699909)
XLA Ops:
  6.6 0.0 all-gather.3.cloned.1.call-start
  6.6 0.7 all-gather.3.cloned.1.call-update
  7.3 0.9 fusion.51
  8.2 0.8 fusion.53
  9.0 0.8 fusion.55
  9.9 0.8 fusion.56
  10.7 20.5 %all-reduce.1 = (f32[1,256]{1,0:T(1,128)S(1)}, f32[2,256]{1,0:T(2,128)S(1)}, f32[2,256]{1,0:T(2,128)S(1)}) all-reduce(f32[1,256]{1,0:T(1,128)S(1)} %fusion.51, f32[2,256]{1,0:T(2,128)S(1)} %fusion.55, f32[2,256]{1,0:T(2,128)S(1)} %fusion.56), channel_id=1, replica_groups=mesh['sp_0'=8,'sp_1'=8,'tp'=8] {'sp_0'}, use_global_device_ids=true, to_apply=%region_4.5 | all-reduce | flops 1280 | bytes 10240 | tf_op jit(solution)/shard_map/psum | solution.py:19
  31.2 14.8 %all-reduce = (f32[1,256]{1,0:T(1,128)S(1)}, f32[2,256]{1,0:T(2,128)S(1)}, f32[2,256]{1,0:T(2,128)S(1)}) all-reduce(f32[1,256]{1,0:T(1,128)S(1)} %get-tuple-element.8, f32[2,256]{1,0:T(2,128)S(1)} %get-tuple-element.9, f32[2,256]{1,0:T(2,128)S(1)} %get-tuple-element.10), channel_id=1, replica_groups=mesh['sp_0'=8,'sp_1'=8,'tp'=8] {'sp_1'}, use_global_device_ids=true, to_apply=%region_5.6 | all-reduce | flops 1280 | bytes 10240 | tf_op jit(solution)/shard_map/psum | solution.py:19
  46.0 20.5 %all_gather.9 = f32[5,2048]{1,0:T(8,128)S(1)} all-gather(f32[5,256]{1,0:T(8,128)S(1)} %pad_maximum_fusion.7), channel_id=1, replica_groups=mesh['sp_0'=8,'sp_1'=8,'tp'=8] {'tp'}, dimensions={1}, use_global_device_ids=true | all-gather | bytes 46080 | tf_op jit(solution)/shard_map/all_gather | solution.py:28
  66.5 1.0 fusion.29
  67.4 0.9 fusion.33
  68.4 0.8 broadcast_in_dim.13
  69.2 3.9 %all-to-all-start = ((bf16[8,16,2048]{2,1,0:T(8,128)(2,1)}), bf16[8,16,2048]{2,1,0:T(8,128)(2,1)S(1)}, u32[]{:S(2)}, u32[]{:S(2)}) async-start(bf16[8,16,2048]{2,1,0:T(8,128)(2,1)} %broadcast_in_dim.13), calls=%async_computation | async-start | bytes 1048576 | tf_op jit(solution)/shard_map/all_to_all | solution.py:33
  73.1 0.9 slice_bitcast_fusion
  74.0 0.1 copy.18
  74.1 0.1 broadcast_multiply_fusion.1
  74.2 0.1 fusion.45
  74.2 8.2 %all-to-all-done = bf16[8,16,2048]{2,1,0:T(8,128)(2,1)S(1)} async-done(((bf16[8,16,2048]{2,1,0:T(8,128)(2,1)}), bf16[8,16,2048]{2,1,0:T(8,128)(2,1)S(1)}, u32[]{:S(2)}, u32[]{:S(2)}) %all-to-all-start) | async-done | bytes 524320 | tf_op jit(solution)/shard_map/all_to_all | solution.py:33
  82.4 0.4 multiply_reduce_fusion.2
  82.9 0.2 fusion.38
  83.1 0.0 copy-done.6
  83.1 0.3 fusion.20
  83.5 0.1 multiply_multiply_fusion
  83.6 0.4 multiply_reduce_fusion.4
  84.0 0.1 multiply_multiply_fusion.1
  84.1 0.3 convolution_convert_fusion.2
  84.3 0.6 pad_maximum_fusion.2
  85.0 0.0 all-gather.5.cloned.1.call-update
  85.0 10.3 %all-gather.3.cloned.1.call-done = bf16[512,2048]{1,0:T(8,128)(2,1)} async-done(((bf16[8,2048]{1,0:T(8,128)(2,1)}), bf16[512,2048]{1,0:T(8,128)(2,1)}) %all-gather.3.cloned.1.call-update) | async-done | bytes 2097168 | tf_op jit(solution)/shard_map/all_gather | solution.py:172
  95.3 2.1 fusion.2
  97.4 2.9 %multiply_reduce_fusion = (f32[512]{0:T(512)S(1)}, f32[512,256]{0,1:T(8,128)S(1)}) fusion(bf16[2048,256]{1,0:T(8,128)(2,1)S(1)} %copy-done, bf16[512,2048]{1,0:T(8,128)(2,1)} %all-gather.3.cloned.1.call-done, f32[2048]{0:T(1024)S(1)} %bitcast.109, f32[2048]{0:T(1024)S(1)} %bitcast.111, f32[2048]{0:T(1024)S(1)} %copy-done.8, f32[512]{0:T(512)S(1)} %add_rsqrt_fusion.2), kind=kOutput, calls=%fused_computation.32 | convolution fusion | flops 543424000 | bytes 3698688 | tf_op jit(solution)/shard_map/dot_general | solution.py:95
  100.3 0.3 fusion.24
  100.6 1.0 fusion.19
  101.6 0.1 multiply_reduce_fusion.1
  101.7 0.4 fusion.66
  102.1 0.3 convolution_convert_fusion.1
  102.4 88.4 %all-gather.5.cloned.1.call-done = bf16[8192,320]{0,1:T(8,128)(2,1)} async-done(((bf16[128,320]{0,1:T(8,128)(2,1)}), bf16[8192,320]{0,1:T(8,128)(2,1)}) %all-gather.5.cloned.1.call-update) | async-done | bytes 5242896 | tf_op jit(solution)/shard_map/all_gather | solution.py:28
  190.8 1.9 slice-done
  192.7 1.4 fusion.67
  194.1 1.4 fusion
  195.5 1.6 slice-done.1
  197.1 1.7 fusion.11
  198.8 0.2 fusion.21
  199.0 0.3 fusion.18
  199.4 0.3 convolution_convert_fusion
  199.7 18.9 %all_to_all.10 = bf16[8,16,2048]{2,1,0:T(8,128)(2,1)S(1)} all-to-all(bf16[8,16,2048]{2,1,0:T(8,128)(2,1)S(1)} %bitcast.99), channel_id=1, replica_groups=mesh['sp_0'=8,'sp_1'=8,'tp'=8] {'tp'}, dimensions={0} | all-to-all | bytes 1048576 | tf_op jit(solution)/shard_map/all_to_all | solution.py:55
  218.6 0.1 convert_reduce_fusion
  218.7 0.7 fusion.34
  (46 shorter events, 0.3 us)
Async XLA Ops:
  6.5 75.9 %copy-start = (bf16[2048,256]{1,0:T(8,128)(2,1)S(1)}, bf16[2048,256]{1,0:T(8,128)(2,1)}, u32[]{:S(2)}) copy-start(bf16[2048,256]{1,0:T(8,128)(2,1)} %param.27) | copy-start | bytes 3145732
  6.5 77.5 %copy-start.5 = (bf16[2,256,128]{2,1,0:T(8,128)(2,1)S(1)}, bf16[2,256,128]{2,1,0:T(8,128)(2,1)}, u32[]{:S(2)}) copy-start(bf16[2,256,128]{2,1,0:T(8,128)(2,1)} %param.30) | copy-start | bytes 393220
  6.5 76.3 %copy-start.7 = (f32[256]{0:T(256)S(1)}, f32[256]{0:T(256)}, u32[]{:S(2)}) copy-start(f32[256]{0:T(256)} %param.29) | copy-start | bytes 3076
  6.5 76.5 %copy-start.6 = (bf16[2048,32]{0,1:T(8,128)(2,1)S(1)}, bf16[2048,32]{0,1:T(8,128)(2,1)}, u32[]{:S(2)}) copy-start(bf16[2048,32]{0,1:T(8,128)(2,1)} %param.28) | copy-start | bytes 393220
  6.5 76.9 %copy-start.10 = (f32[96]{0:T(128)S(1)}, f32[96]{0:T(128)}, u32[]{:S(2)}) copy-start(f32[96]{0:T(128)} %param.31) | copy-start | bytes 1156
  6.5 77.0 %copy-start.2 = (bf16[2048,192]{0,1:T(8,128)(2,1)S(1)}, bf16[2048,192]{0,1:T(8,128)(2,1)}, u32[]{:S(2)}) copy-start(bf16[2048,192]{0,1:T(8,128)(2,1)} %param.25) | copy-start | bytes 2359300
  6.6 77.4 %copy-start.9 = (f32[96]{0:T(128)S(1)}, f32[96]{0:T(128)}, u32[]{:S(2)}) copy-start(f32[96]{0:T(128)} %param.26) | copy-start | bytes 1156
  6.6 88.7 %all-gather.3.cloned.1.call-start = ((), (), s32[]{:S(2)}) async-start(), calls=%async_computation.2 | async-start | bytes 2129920 | tf_op jit(solution)/shard_map/all_gather | solution.py:172
  69.2 13.2 %all-to-all-start = ((bf16[8,16,2048]{2,1,0:T(8,128)(2,1)}), bf16[8,16,2048]{2,1,0:T(8,128)(2,1)S(1)}, u32[]{:S(2)}, u32[]{:S(2)}) async-start(bf16[8,16,2048]{2,1,0:T(8,128)(2,1)} %broadcast_in_dim.13), calls=%async_computation | async-start | bytes 1048576 | tf_op jit(solution)/shard_map/all_to_all | solution.py:33
  73.1 24.3 %copy-start.8 = (f32[2048]{0:T(1024)S(1)}, f32[2048]{0:T(1024)}, u32[]{:S(2)}) copy-start(f32[2048]{0:T(1024)} %param.24) | copy-start | bytes 24580
  73.1 117.7 %all-gather.5.cloned.1.call-start = ((), (), s32[]{:S(2)}) async-start(), calls=%async_computation.3 | async-start | bytes 5324800 | tf_op jit(solution)/shard_map/all_gather | solution.py:28
  97.4 3.2 %copy-start.1 = (bf16[512,2048]{1,0:T(8,128)(2,1)S(1)}, bf16[512,2048]{1,0:T(8,128)(2,1)}, u32[]{:S(2)}) copy-start(bf16[512,2048]{1,0:T(8,128)(2,1)} %all-gather.3.cloned.1.call-done) | copy-start | bytes 6291460
  100.3 1.4 copy-start.11
  190.8 1.9 slice-start
  195.5 1.6 slice-start.1
  197.1 2.3 %copy-start.4 = (bf16[128,2048]{1,0:T(8,128)(2,1)S(1)}, bf16[128,2048]{1,0:T(8,128)(2,1)}, u32[]{:S(2)}) copy-start(bf16[128,2048]{1,0:T(8,128)(2,1)} %param.33) | copy-start | bytes 1572868
  197.1 21.6 %copy-start.3 = (bf16[16,2048]{1,0:T(8,128)(2,1)S(1)}, bf16[16,2048]{1,0:T(8,128)(2,1)}, u32[]{:S(2)}) copy-start(bf16[16,2048]{1,0:T(8,128)(2,1)} %param.17) | copy-start | bytes 196612
Sparse Core Ops, SparseCore 0:
  10.4 84.8 all-gather.2
  98.3 92.4 all-gather.4
where the time goes:
time: 227 us; the launch traced here: 226 us
  waiting for transfers between devices  108 us (48%)
  blocking collectives  74.6 us (33%)
  between operations  13.7 us (6%)
  matrix products  12.7 us (6%)
  other arithmetic  8.28 us (4%)
  local copies, waits for them, and re-layouts  5.41 us (2%)
  starting transfers between devices  3.9 us (2%)
    all_gather x1, waiting for transfers between devices, in_one_piece(): lax.all_gather(both, axis, axis=dim, tiled=True)  88.4 us
    psum x2, blocking collectives, over_axes(): return functools.reduce(lax.psum, axes, value)  35.2 us
    all_gather x1, blocking collectives, in_one_piece(): lax.all_gather(both, axis, axis=dim, tiled=True)  20.5 us
    all_to_all x1, blocking collectives, sent_and_summed(): tiles = lax.all_to_all(split_up(value, dim, count), axis, 0, 0, tiled=True)  18.9 us
    all_gather x1, waiting for transfers between devices, local(): ctx_rows = lax.all_gather(context_tokens, SP, axis=0, tiled=True)  10.3 us
    all_to_all x1, waiting for transfers between devices, copy_for_each(): return lax.all_to_all(copies, axis, split_axis=0, concat_axis=0, tiled=True)  8.21 us
  transfers between devices with their start and end apart: 3, of which 3 were waited for; matrix products, arithmetic and copies ran while one was open for 7% of the time, Pallas kernels for 0%

commit v1 on v0

--- a/solution.py
+++ b/solution.py
@@ -169,7 +169,9 @@
     hidden_lat = (
         rms_normed(latent_tokens, norm_gain) * (1.0 + scale_vec[0]) + shift_vec[0]
     ).astype(jnp.bfloat16)
-    ctx_rows = lax.all_gather(context_tokens, SP, axis=0, tiled=True)
+    ctx_rows = jnp.concatenate(
+        lax.all_to_all(jnp.stack([context_tokens] * lax.axis_size(SP)), SP, 0, 0), axis=0
+    )
     ctx_hidden = (rms_normed(ctx_rows, norm_gain) * (1.0 + scale_vec[1]) + shift_vec[1]).astype(
         jnp.bfloat16
     )

time: 227 us -> 246 us (1.084)
  waiting for transfers between devices: 108 us -> 120 us
  starting transfers between devices: 3.9 us -> 9.8 us
    all_to_all x0 -> x1, waiting for transfers between devices: none -> 52.5 us  [local(): lax.all_to_all(jnp.stack([context_tokens] * lax.axis_size(SP)), SP, 0, 0)]
    all_gather x1, waiting for transfers between devices: 88.4 us -> 59.2 us  [in_one_piece(): lax.all_gather(both, axis, axis=dim, tiled=True)]
    all_gather x1 -> x0, waiting for transfers between devices: 10.3 us -> none  [local(): ctx_rows = lax.all_gather(context_tokens, SP, axis=0, tiled=True)]
    all_to_all x0 -> x1, starting transfers between devices: none -> 5.94 us  [local(): lax.all_to_all(jnp.stack([context_tokens] * lax.axis_size(SP)), SP, 0, 0)]
  transfers between devices with their start and end apart: 3 -> 3, of which waited for: 3 -> 3; matrix products, arithmetic and copies ran while one was open for 7% -> 3% of each run, Pallas kernels for 0% -> 0%
where the time goes in v1:
time: 246 us; the launch traced here: 245 us
  waiting for transfers between devices  120 us (49%)
  blocking collectives  74.6 us (30%)
  between operations  13.7 us (6%)
  matrix products  13 us (5%)
  starting transfers between devices  9.8 us (4%)
  local copies, waits for them, and re-layouts  7.12 us (3%)
  other arithmetic  6.78 us (3%)
    all_gather x1, waiting for transfers between devices, in_one_piece(): lax.all_gather(both, axis, axis=dim, tiled=True)  59.2 us
    all_to_all x1, waiting for transfers between devices, local(): lax.all_to_all(jnp.stack([context_tokens] * lax.axis_size(SP)), SP, 0, 0)  52.5 us
    psum x2, blocking collectives, over_axes(): return functools.reduce(lax.psum, axes, value)  34.5 us
    all_gather x1, blocking collectives, in_one_piece(): lax.all_gather(both, axis, axis=dim, tiled=True)  21.1 us
    all_to_all x1, blocking collectives, sent_and_summed(): tiles = lax.all_to_all(split_up(value, dim, count), axis, 0, 0, tiled=True)  18.9 us
    all_to_all x1, waiting for transfers between devices, copy_for_each(): return lax.all_to_all(copies, axis, split_axis=0, concat_axis=0, tiled=True)  8.23 us
    all_to_all x1, starting transfers between devices, local(): lax.all_to_all(jnp.stack([context_tokens] * lax.axis_size(SP)), SP, 0, 0)  5.94 us
  transfers between devices with their start and end apart: 3, of which 3 were waited for; matrix products, arithmetic and copies ran while one was open for 3% of the time, Pallas kernels for 0%

profile of v1, /device:TPU:1, one launch (start us, length us, event | category | flops | bytes accessed | tf_op | source)
XLA Modules:
  0.0 244.9 jit_solution(8070435181512765253)
XLA Ops:
  6.6 1.1 fusion.30
  7.6 0.9 fusion.52
  8.6 0.8 fusion.54
  9.4 0.8 fusion.56
  10.2 0.8 fusion.57
  11.0 20.5 %all-reduce.1 = (f32[1,256]{1,0:T(1,128)S(1)}, f32[2,256]{1,0:T(2,128)S(1)}, f32[2,256]{1,0:T(2,128)S(1)}) all-reduce(f32[1,256]{1,0:T(1,128)S(1)} %fusion.52, f32[2,256]{1,0:T(2,128)S(1)} %fusion.56, f32[2,256]{1,0:T(2,128)S(1)} %fusion.57), channel_id=1, replica_groups=mesh['sp_0'=8,'sp_1'=8,'tp'=8] {'sp_0'}, use_global_device_ids=true, to_apply=%region_4.5 | all-reduce | flops 1280 | bytes 10240 | tf_op jit(solution)/shard_map/psum | solution.py:19
  31.5 14.1 %all-reduce = (f32[1,256]{1,0:T(1,128)S(1)}, f32[2,256]{1,0:T(2,128)S(1)}, f32[2,256]{1,0:T(2,128)S(1)}) all-reduce(f32[1,256]{1,0:T(1,128)S(1)} %get-tuple-element.8, f32[2,256]{1,0:T(2,128)S(1)} %get-tuple-element.9, f32[2,256]{1,0:T(2,128)S(1)} %get-tuple-element.10), channel_id=1, replica_groups=mesh['sp_0'=8,'sp_1'=8,'tp'=8] {'sp_1'}, use_global_device_ids=true, to_apply=%region_5.6 | all-reduce | flops 1280 | bytes 10240 | tf_op jit(solution)/shard_map/psum | solution.py:19
  45.6 21.1 %all_gather.6 = f32[5,2048]{1,0:T(8,128)S(1)} all-gather(f32[5,256]{1,0:T(8,128)S(1)} %pad_maximum_fusion.7), channel_id=1, replica_groups=mesh['sp_0'=8,'sp_1'=8,'tp'=8] {'tp'}, dimensions={1}, use_global_device_ids=true | all-gather | bytes 46080 | tf_op jit(solution)/shard_map/all_gather | solution.py:28
  66.8 0.9 fusion.34
  67.7 0.8 broadcast_in_dim.13
  68.6 3.9 %all-to-all-start = ((bf16[8,16,2048]{2,1,0:T(8,128)(2,1)}), bf16[8,16,2048]{2,1,0:T(8,128)(2,1)S(1)}, u32[]{:S(2)}, u32[]{:S(2)}) async-start(bf16[8,16,2048]{2,1,0:T(8,128)(2,1)} %broadcast_in_dim.13), calls=%async_computation | async-start | bytes 1048576 | tf_op jit(solution)/shard_map/all_to_all | solution.py:33
  72.4 0.8 slice_bitcast_fusion
  73.3 0.1 copy.22
  73.4 0.1 broadcast_multiply_fusion.1
  73.5 0.1 fusion.46
  73.6 8.2 %all-to-all-done = bf16[8,16,2048]{2,1,0:T(8,128)(2,1)S(1)} async-done(((bf16[8,16,2048]{2,1,0:T(8,128)(2,1)}), bf16[8,16,2048]{2,1,0:T(8,128)(2,1)S(1)}, u32[]{:S(2)}, u32[]{:S(2)}) %all-to-all-start) | async-done | bytes 524320 | tf_op jit(solution)/shard_map/all_to_all | solution.py:33
  81.8 1.5 multiply_reduce_fusion.4
  83.3 1.2 fusion.21
  84.5 0.4 multiply_reduce_fusion.2
  84.9 0.2 convolution_convert_fusion.2
  85.2 0.2 fusion.39
  85.5 0.1 multiply_multiply_fusion
  85.6 0.1 multiply_multiply_fusion.1
  85.7 0.6 pad_maximum_fusion.2
  86.4 0.0 all-gather.2.cloned.1.call-update
  86.4 1.6 stack.11
  88.0 5.9 %all-to-all-start.1 = ((bf16[64,8,2048]{2,1,0:T(8,128)(2,1)}), bf16[64,8,2048]{2,1,0:T(8,128)(2,1)S(1)}, u32[]{:S(2)}, u32[]{:S(2)}) async-start(bf16[64,8,2048]{2,1,0:T(8,128)(2,1)} %stack.11), calls=%async_computation.1 | async-start | bytes 4194304 | tf_op jit(solution)/shard_map/all_to_all | solution.py:173
  94.0 52.5 %all-to-all-done.1 = bf16[64,8,2048]{2,1,0:T(8,128)(2,1)S(1)} async-done(((bf16[64,8,2048]{2,1,0:T(8,128)(2,1)}), bf16[64,8,2048]{2,1,0:T(8,128)(2,1)S(1)}, u32[]{:S(2)}, u32[]{:S(2)}) %all-to-all-start.1) | async-done | bytes 2097184 | tf_op jit(solution)/shard_map/all_to_all | solution.py:173
  146.5 0.5 fusion.7
  147.0 0.1 rsqrt.62
  147.1 1.2 multiply_reduce_fusion
  148.3 0.3 fusion.25
  148.6 1.0 fusion.20
  149.6 0.1 multiply_reduce_fusion.1
  149.7 0.4 fusion.67
  150.0 0.3 convolution_convert_fusion.1
  150.3 59.2 %all-gather.2.cloned.1.call-done = bf16[8192,320]{0,1:T(8,128)(2,1)} async-done(((bf16[128,320]{0,1:T(8,128)(2,1)}), bf16[8192,320]{0,1:T(8,128)(2,1)}) %all-gather.2.cloned.1.call-update) | async-done | bytes 5242896 | tf_op jit(solution)/shard_map/all_gather | solution.py:28
  209.5 1.9 slice-done
  211.4 1.4 fusion.68
  212.8 1.4 fusion
  214.2 1.6 slice-done.1
  215.8 1.7 fusion.12
  217.5 0.2 fusion.22
  217.8 0.3 fusion.19
  218.1 0.3 convolution_convert_fusion
  218.4 18.9 %all_to_all.15 = bf16[8,16,2048]{2,1,0:T(8,128)(2,1)S(1)} all-to-all(bf16[8,16,2048]{2,1,0:T(8,128)(2,1)S(1)} %bitcast.115), channel_id=1, replica_groups=mesh['sp_0'=8,'sp_1'=8,'tp'=8] {'tp'}, dimensions={0} | all-to-all | bytes 1048576 | tf_op jit(solution)/shard_map/all_to_all | solution.py:55
  237.3 0.1 convert_reduce_fusion
  237.4 0.7 fusion.35
  (45 shorter events, 0.3 us)
Async XLA Ops:
  6.5 78.0 %copy-start = (bf16[2048,256]{1,0:T(8,128)(2,1)S(1)}, bf16[2048,256]{1,0:T(8,128)(2,1)}, u32[]{:S(2)}) copy-start(bf16[2048,256]{1,0:T(8,128)(2,1)} %param.27) | copy-start | bytes 3145732
  6.5 78.4 %copy-start.3 = (bf16[2,256,128]{2,1,0:T(8,128)(2,1)S(1)}, bf16[2,256,128]{2,1,0:T(8,128)(2,1)}, u32[]{:S(2)}) copy-start(bf16[2,256,128]{2,1,0:T(8,128)(2,1)} %param.30) | copy-start | bytes 393220
  6.5 78.4 %copy-start.6 = (f32[256]{0:T(256)S(1)}, f32[256]{0:T(256)}, u32[]{:S(2)}) copy-start(f32[256]{0:T(256)} %param.29) | copy-start | bytes 3076
  6.5 78.9 %copy-start.9 = (f32[96]{0:T(128)S(1)}, f32[96]{0:T(128)}, u32[]{:S(2)}) copy-start(f32[96]{0:T(128)} %param.31) | copy-start | bytes 1156
  6.5 79.1 %copy-start.8 = (f32[96]{0:T(128)S(1)}, f32[96]{0:T(128)}, u32[]{:S(2)}) copy-start(f32[96]{0:T(128)} %param.26) | copy-start | bytes 1156
  6.5 79.8 %copy-start.5 = (bf16[8,2048]{1,0:T(8,128)(2,1)S(1)}, bf16[8,2048]{1,0:T(8,128)(2,1)}, u32[]{:S(2)}) copy-start(bf16[8,2048]{1,0:T(8,128)(2,1)} %param.18) | copy-start | bytes 98308
  68.6 13.2 %all-to-all-start = ((bf16[8,16,2048]{2,1,0:T(8,128)(2,1)}), bf16[8,16,2048]{2,1,0:T(8,128)(2,1)S(1)}, u32[]{:S(2)}, u32[]{:S(2)}) async-start(bf16[8,16,2048]{2,1,0:T(8,128)(2,1)} %broadcast_in_dim.13), calls=%async_computation | async-start | bytes 1048576 | tf_op jit(solution)/shard_map/all_to_all | solution.py:33
  72.4 137.1 %all-gather.2.cloned.1.call-start = ((), (), s32[]{:S(2)}) async-start(), calls=%async_computation.3 | async-start | bytes 5324800 | tf_op jit(solution)/shard_map/all_gather | solution.py:28
  86.4 60.7 %copy-start.7 = (f32[2048]{0:T(1024)S(1)}, f32[2048]{0:T(1024)}, u32[]{:S(2)}) copy-start(f32[2048]{0:T(1024)} %param.24) | copy-start | bytes 24580
  88.0 58.4 %all-to-all-start.1 = ((bf16[64,8,2048]{2,1,0:T(8,128)(2,1)}), bf16[64,8,2048]{2,1,0:T(8,128)(2,1)S(1)}, u32[]{:S(2)}, u32[]{:S(2)}) async-start(bf16[64,8,2048]{2,1,0:T(8,128)(2,1)} %stack.11), calls=%async_computation.1 | async-start | bytes 4194304 | tf_op jit(solution)/shard_map/all_to_all | solution.py:173
  147.1 1.5 copy-start.4
  148.3 1.4 copy-start.10
  209.5 1.9 slice-start
  214.2 1.6 slice-start.1
  215.8 2.3 copy-start.2
  215.8 21.6 %copy-start.1 = (bf16[16,2048]{1,0:T(8,128)(2,1)S(1)}, bf16[16,2048]{1,0:T(8,128)(2,1)}, u32[]{:S(2)}) copy-start(bf16[16,2048]{1,0:T(8,128)(2,1)} %param.17) | copy-start | bytes 196612
Sparse Core Ops, SparseCore 0:
  86.5 122.9 all-gather.1
